TPU v7x, 32 devices: a whole 2x2x4 slice. The times are simulated.
32 devices in a mesh: fs: 4 (over y, x), tp: 8 (over z, core).
Axes of the slice: x: 2, y: 2, z: 4, core: 2. Of those that a mesh axis runs over, the one named last changes fastest.
Arguments:
- tokens: bfloat16 [4096, 2048], P(('fs', 'tp')), may hold values from -6 to 6
- norm_gain: float32 [2048], replicated, may hold values from 0.1 to 1.9
- gate_weight: bfloat16 [2048, 5632], P('fs', 'tp'), may hold values from -0.125 to 0.125
- up_weight: bfloat16 [2048, 5632], P('fs', 'tp'), may hold values from -0.125 to 0.125
- down_weight: bfloat16 [5632, 2048], P('tp', 'fs'), may hold values from -0.078125 to 0.078125
Outputs:
- mixed: bfloat16 [4096, 2048], P(('fs', 'tp'))
All inputs are finite; a program needn't handle non-finite values.
Results may differ from a plain program's by a relative error of at most 0.0065.
Values may be sent and summed in bfloat16 or wider, within the bound.
A program may use at most 128 MiB of HBM per device.

v0:
```python
import jax
import jax.numpy as jnp
from jax import lax
from jax.sharding import PartitionSpec as P

eps_floor = 0.05


def local(tokens, norm_gain, gate_weight, up_weight, down_weight):
    values = tokens.astype(jnp.float32)
    factor = lax.rsqrt(jnp.mean(values * values, axis=-1, keepdims=True) + eps_floor)
    normed = (values * factor * norm_gain).astype(jnp.bfloat16)
    local_ff = gate_weight.shape[1]
    group = lax.all_gather(normed, "tp", axis=0, tiled=True)
    joined = jnp.concatenate(
        (
            lax.all_gather(gate_weight, "fs", axis=0, tiled=True),
            lax.all_gather(up_weight, "fs", axis=0, tiled=True),
        ),
        axis=1,
    )
    product = jnp.dot(group, joined, preferred_element_type=jnp.float32)
    hidden = (jax.nn.silu(product[:, :local_ff]) * product[:, local_ff:]).astype(jnp.bfloat16)
    down_local = lax.all_gather(down_weight, "fs", axis=1, tiled=True)
    mixed = lax.psum_scatter(
        jnp.dot(hidden, down_local, preferred_element_type=jnp.float32),
        "tp",
        scatter_dimension=0,
        tiled=True,
    )
    return mixed.astype(jnp.bfloat16)


def solution(mesh):
    return jax.shard_map(
        local,
        mesh=mesh,
        in_specs=(P(("fs", "tp"), None), P(), P("fs", "tp"), P("fs", "tp"), P("tp", "fs")),
        out_specs=P(("fs", "tp"), None),
        check_vma=False,
    )
```

profile of v0, /device:TPU:0, one launch (start us, length us, event | category | flops | bytes accessed | tf_op | source)
XLA Modules:
  0.0 296.1 jit_solution(4076748041551358290)
XLA Ops:
  6.5 0.0 all-gather.7.cloned.1.call-start
  6.5 0.7 all-gather.7.cloned.1.call-update
  7.3 0.0 all-gather.9.cloned.1.call-start
  7.3 0.7 all-gather.9.cloned.1.call-update
  8.0 0.0 all-gather.5.cloned.1.call-start
  8.1 1.2 fusion.8
  9.3 2.0 fusion.10
  11.3 0.0 all-gather.5.cloned.1.call-update
  11.3 0.0 all-gather.11.cloned.1.call-start
  11.4 0.5 all-gather.11.cloned.1.call-update
  11.9 0.0 reduce-scatter.2.cloned.1.call-start
  12.0 41.5 %all-gather.7.cloned.1.call-done = bf16[2048,704]{0,1:T(8,128)(2,1)} async-done(((bf16[512,704]{0,1:T(8,128)(2,1)}), bf16[2048,704]{0,1:T(8,128)(2,1)}) %all-gather.7.cloned.1.call-update) | async-done | bytes 2883600 | tf_op jit(solution)/shard_map/all_gather | solution.py:17
  53.5 43.4 %all-gather.9.cloned.1.call-done = bf16[2048,704]{0,1:T(8,128)(2,1)} async-done(((bf16[512,704]{0,1:T(8,128)(2,1)}), bf16[2048,704]{0,1:T(8,128)(2,1)}) %all-gather.9.cloned.1.call-update) | async-done | bytes 2883600 | tf_op jit(solution)/shard_map/all_gather | solution.py:18
  96.9 48.5 %all-gather.5.cloned.1.call-done = bf16[1024,2048]{1,0:T(8,128)(2,1)} async-done(((bf16[128,2048]{1,0:T(8,128)(2,1)}), bf16[1024,2048]{1,0:T(8,128)(2,1)}) %all-gather.5.cloned.1.call-update) | async-done | bytes 4194320 | tf_op jit(solution)/shard_map/all_gather | solution.py:14
  145.4 11.8 %fusion = f32[1024,1408]{1,0:T(8,128)} fusion(bf16[1024,2048]{1,0:T(8,128)(2,1)} %all-gather.5.cloned.1.call-done, bf16[2048,704]{0,1:T(8,128)(2,1)} %all-gather.9.cloned.1.call-done, bf16[2048,704]{0,1:T(8,128)(2,1)} %all-gather.7.cloned.1.call-done), kind=kOutput, calls=%fused_computation | convolution fusion | flops 5917114368 | bytes 15728640 | tf_op jit(solution)/shard_map/dot_general | solution.py:22
  157.2 30.2 %all-gather.11.cloned.1.call-done = bf16[704,2048]{1,0:T(8,128)(2,1)} async-done(((bf16[704,512]{1,0:T(8,128)(2,1)}), bf16[704,2048]{1,0:T(8,128)(2,1)}) %all-gather.11.cloned.1.call-update) | async-done | bytes 2883600 | tf_op jit(solution)/shard_map/all_gather | solution.py:24
  187.4 10.4 %fusion.5 = f32[1024,2048]{1,0:T(8,128)} fusion(bf16[704,2048]{1,0:T(8,128)(2,1)} %all-gather.11.cloned.1.call-done, f32[1024,1408]{1,0:T(8,128)} %fusion), kind=kOutput, calls=%fused_computation.6 | convolution fusion | flops 2957115392 | bytes 17563648 | tf_op jit(solution)/shard_map/dot_general | solution.py:26
  197.8 0.0 reduce-scatter.2.cloned.1.call-update
  197.8 89.7 %reduce-scatter.2.cloned.1.call-done = f32[128,2048]{1,0:T(8,128)} async-done(((f32[1024,2048]{1,0:T(8,128)}), f32[128,2048]{1,0:T(8,128)}) %reduce-scatter.2.cloned.1.call-update) | async-done | bytes 1048592 | tf_op jit(solution)/shard_map/reduce_scatter | solution.py:25
  287.5 2.1 convert_element_type.15
  (1 shorter events, 0.0 us)
Async XLA Ops:
  6.5 46.9 %all-gather.7.cloned.1.call-start = ((), (), s32[]{:S(2)}) async-start(), calls=%async_computation.2 | async-start | bytes 3604480 | tf_op jit(solution)/shard_map/all_gather | solution.py:17
  7.3 89.6 %all-gather.9.cloned.1.call-start = ((), (), s32[]{:S(2)}) async-start(), calls=%async_computation.3 | async-start | bytes 3604480 | tf_op jit(solution)/shard_map/all_gather | solution.py:18
  8.0 137.3 %all-gather.5.cloned.1.call-start = ((), (), s32[]{:S(2)}) async-start(), calls=%async_computation.1 | async-start | bytes 4718592 | tf_op jit(solution)/shard_map/all_gather | solution.py:14
  11.3 176.1 %all-gather.11.cloned.1.call-start = ((), (), s32[]{:S(2)}) async-start(), calls=%async_computation.4 | async-start | bytes 3604480 | tf_op jit(solution)/shard_map/all_gather | solution.py:24
  11.9 275.6 %reduce-scatter.2.cloned.1.call-start = ((), (), s32[]{:S(2)}) async-start(), calls=%async_computation.5 | async-start | bytes 9437184 | tf_op jit(solution)/shard_map/reduce_scatter | solution.py:25
Sparse Core Ops, SparseCore 0:
  9.2 44.2 all-gather.6
  55.3 41.5 all-gather.8
  98.5 46.8 all-gather.4
  147.0 40.3 all-gather.10
  198.0 89.5 reduce-scatter.1
where the time goes:
time: 296 us
  waiting for transfers between devices  255 us (86%)
  matrix products  22.2 us (8%)
  between operations  13.1 us (4%)
  other arithmetic  5.35 us (2%)
    reduce_scatter x1, waiting for transfers between devices, local(): lax.psum_scatter(jnp.dot(hidden, down_local, preferred_element_type=jnp.f...  89.7 us
    all_gather x1, waiting for transfers between devices, local(): group = lax.all_gather(normed, 'tp', axis=0, tiled=True)  48.5 us
    all_gather x1, waiting for transfers between devices, local(): lax.all_gather(up_weight, 'fs', axis=0, tiled=True)  43.4 us
    all_gather x1, waiting for transfers between devices, local(): lax.all_gather(gate_weight, 'fs', axis=0, tiled=True)  41.5 us
    all_gather x1, waiting for transfers between devices, local(): down_local = lax.all_gather(down_weight, 'fs', axis=1, tiled=True)  30.2 us
    dot_general x1, matrix products, local(): product = jnp.dot(group, joined, preferred_element_type=jnp.float32)  11.8 us
    dot_general x1, matrix products, local(): jnp.dot(hidden, down_local, preferred_element_type=jnp.float32)  10.4 us
  transfers between devices with their start and end apart: 5, of which 5 were waited for; matrix products, arithmetic and copies ran while one was open for 5% of the time, Pallas kernels for 0%

commit v1 on v0

--- a/solution.py
+++ b/solution.py
@@ -21,7 +21,9 @@
     )
     product = jnp.dot(group, joined, preferred_element_type=jnp.float32)
     hidden = (jax.nn.silu(product[:, :local_ff]) * product[:, local_ff:]).astype(jnp.bfloat16)
-    down_local = lax.all_gather(down_weight, "fs", axis=1, tiled=True)
+    down_local = jnp.concatenate(
+        lax.all_to_all(jnp.stack([down_weight] * lax.axis_size("fs")), "fs", 0, 0), axis=1
+    )
     mixed = lax.psum_scatter(
         jnp.dot(hidden, down_local, preferred_element_type=jnp.float32),
         "tp",

time: 296 us -> 279 us (0.943)
  waiting for transfers between devices: 255 us -> 192 us
  blocking collectives: 0 us -> 51.5 us
  matrix products: 22.2 us -> 16.6 us
    all_to_all x0 -> x1, blocking collectives: none -> 51.5 us  [local(): lax.all_to_all(jnp.stack([down_weight] * lax.axis_size('fs')), 'fs', 0, 0)]
    all_gather x1, waiting for transfers between devices: 41.5 us -> 9.73 us  [local(): lax.all_gather(gate_weight, 'fs', axis=0, tiled=True)]
    all_gather x1 -> x0, waiting for transfers between devices: 30.2 us -> none  [local(): down_local = lax.all_gather(down_weight, 'fs', axis=1, tiled=True)]
    dot_general x1, matrix products: 10.4 us -> 5.83 us  [local(): jnp.dot(hidden, down_local, preferred_element_type=jnp.float32)]
  transfers between devices with their start and end apart: 5 -> 4, of which waited for: 5 -> 4; matrix products, arithmetic and copies ran while one was open for 5% -> 1% of each run, Pallas kernels for 0% -> 0%
where the time goes in v1:
time: 279 us
  waiting for transfers between devices  192 us (69%)
  blocking collectives  51.5 us (18%)
  matrix products  16.6 us (6%)
  between operations  13.2 us (5%)
  other arithmetic  5.35 us (2%)
    reduce_scatter x1, waiting for transfers between devices, local(): lax.psum_scatter(jnp.dot(hidden, down_local, preferred_element_type=jnp.f...  88.5 us
    all_to_all x1, blocking collectives, local(): lax.all_to_all(jnp.stack([down_weight] * lax.axis_size('fs')), 'fs', 0, 0)  51.5 us
    all_gather x1, waiting for transfers between devices, local(): group = lax.all_gather(normed, 'tp', axis=0, tiled=True)  48.5 us
    all_gather x1, waiting for transfers between devices, local(): lax.all_gather(up_weight, 'fs', axis=0, tiled=True)  43.7 us
    dot_general x1, matrix products, local(): product = jnp.dot(group, joined, preferred_element_type=jnp.float32)  10.8 us
    all_gather x1, waiting for transfers between devices, local(): lax.all_gather(gate_weight, 'fs', axis=0, tiled=True)  9.73 us
    dot_general x1, matrix products, local(): jnp.dot(hidden, down_local, preferred_element_type=jnp.float32)  5.83 us
  transfers between devices with their start and end apart: 4, of which 4 were waited for; matrix products, arithmetic and copies ran while one was open for 1% of the time, Pallas kernels for 0%

profile of v1, /device:TPU:0, one launch (start us, length us, event | category | flops | bytes accessed | tf_op | source)
XLA Modules:
  0.0 279.2 jit_solution(14670812214996396466)
XLA Ops:
  6.5 0.0 copy-start
  6.5 0.0 all-gather.6.cloned.1.call-start
  6.5 0.7 all-gather.6.cloned.1.call-update
  7.3 0.0 all-gather.8.cloned.1.call-start
  7.3 0.7 all-gather.8.cloned.1.call-update
  8.0 0.0 all-gather.4.cloned.1.call-start
  8.1 1.2 fusion.8
  9.3 2.0 fusion.10
  11.3 0.0 all-gather.4.cloned.1.call-update
  11.3 0.0 reduce-scatter.2.cloned.1.call-start
  11.4 0.0 copy-done
  11.4 0.2 stack.2
  11.6 51.5 %all_to_all.5 = bf16[4,704,512]{2,1,0:T(8,128)(2,1)S(1)} all-to-all(bf16[4,704,512]{2,1,0:T(8,128)(2,1)S(1)} %stack.2), channel_id=1, replica_groups=mesh['fs'=4,'tp'=8] {'fs'}, dimensions={0} | all-to-all | bytes 5767168 | tf_op jit(solution)/shard_map/all_to_all | solution.py:25
  63.1 0.4 copy.7
  63.6 9.7 %all-gather.6.cloned.1.call-done = bf16[2048,704]{0,1:T(8,128)(2,1)} async-done(((bf16[512,704]{0,1:T(8,128)(2,1)}), bf16[2048,704]{0,1:T(8,128)(2,1)}) %all-gather.6.cloned.1.call-update) | async-done | bytes 2883600 | tf_op jit(solution)/shard_map/all_gather | solution.py:17
  73.3 43.7 %all-gather.8.cloned.1.call-done = bf16[2048,704]{0,1:T(8,128)(2,1)} async-done(((bf16[512,704]{0,1:T(8,128)(2,1)}), bf16[2048,704]{0,1:T(8,128)(2,1)}) %all-gather.8.cloned.1.call-update) | async-done | bytes 2883600 | tf_op jit(solution)/shard_map/all_gather | solution.py:18
  117.0 48.5 %all-gather.4.cloned.1.call-done = bf16[1024,2048]{1,0:T(8,128)(2,1)} async-done(((bf16[128,2048]{1,0:T(8,128)(2,1)}), bf16[1024,2048]{1,0:T(8,128)(2,1)}) %all-gather.4.cloned.1.call-update) | async-done | bytes 4194320 | tf_op jit(solution)/shard_map/all_gather | solution.py:14
  165.5 10.8 %fusion = f32[1024,1408]{1,0:T(8,128)S(1)} fusion(bf16[1024,2048]{1,0:T(8,128)(2,1)} %all-gather.4.cloned.1.call-done, bf16[2048,704]{0,1:T(8,128)(2,1)} %all-gather.8.cloned.1.call-done, bf16[2048,704]{0,1:T(8,128)(2,1)} %all-gather.6.cloned.1.call-done), kind=kOutput, calls=%fused_computation | convolution fusion | flops 5917114368 | bytes 15728640 | tf_op jit(solution)/shard_map/dot_general | solution.py:22
  176.2 5.8 %fusion.5 = f32[1024,2048]{1,0:T(8,128)} fusion(bf16[704,2048]{1,0:T(8,128)(2,1)S(1)} %bitcast.6, f32[1024,1408]{1,0:T(8,128)S(1)} %fusion), kind=kOutput, calls=%fused_computation.6 | convolution fusion | flops 2957115392 | bytes 17563648 | tf_op jit(solution)/shard_map/dot_general | solution.py:28
  182.1 0.0 reduce-scatter.2.cloned.1.call-update
  182.1 88.5 %reduce-scatter.2.cloned.1.call-done = f32[128,2048]{1,0:T(8,128)} async-done(((f32[1024,2048]{1,0:T(8,128)}), f32[128,2048]{1,0:T(8,128)}) %reduce-scatter.2.cloned.1.call-update) | async-done | bytes 1048592 | tf_op jit(solution)/shard_map/reduce_scatter | solution.py:27
  270.6 2.1 convert_element_type.15
  (1 shorter events, 0.0 us)
Async XLA Ops:
  6.5 4.9 %copy-start = (bf16[704,512]{1,0:T(8,128)(2,1)S(1)}, bf16[704,512]{1,0:T(8,128)(2,1)}, u32[]{:S(2)}) copy-start(bf16[704,512]{1,0:T(8,128)(2,1)} %param.9) | copy-start | bytes 2162692
  6.5 66.8 %all-gather.6.cloned.1.call-start = ((), (), s32[]{:S(2)}) async-start(), calls=%async_computation.3 | async-start | bytes 3604480 | tf_op jit(solution)/shard_map/all_gather | solution.py:17
  7.3 109.7 %all-gather.8.cloned.1.call-start = ((), (), s32[]{:S(2)}) async-start(), calls=%async_computation.4 | async-start | bytes 3604480 | tf_op jit(solution)/shard_map/all_gather | solution.py:18
  8.0 157.5 %all-gather.4.cloned.1.call-start = ((), (), s32[]{:S(2)}) async-start(), calls=%async_computation.2 | async-start | bytes 4718592 | tf_op jit(solution)/shard_map/all_gather | solution.py:14
  11.3 259.2 %reduce-scatter.2.cloned.1.call-start = ((), (), s32[]{:S(2)}) async-start(), calls=%async_computation.5 | async-start | bytes 9437184 | tf_op jit(solution)/shard_map/reduce_scatter | solution.py:27
Sparse Core Ops, SparseCore 0:
  9.2 64.1 all-gather.5
  75.1 41.7 all-gather.7
  118.6 46.8 all-gather.3
  182.2 88.3 reduce-scatter.1
